TPU v7x, 32 devices: a whole 2x2x4 slice. The times are simulated.
32 devices in a mesh: kv: 16 (over z, y, x), tp: 2 (over core).
Axes of the slice: x: 2, y: 2, z: 4, core: 2. Of those that a mesh axis runs over, the one named last changes fastest.
Arguments:
- residual_in: bfloat16 [96, 2048], P('kv', 'tp'), may hold values from -36 to 36
- gain_pre: float32 [2048], P('tp'), may hold values from 0.1 to 1.9
- gate_pre: bfloat16 [2048, 5632], P('tp', 'kv'), may hold values from -0.125 to 0.125
- up_pre: bfloat16 [2048, 5632], P('tp', 'kv'), may hold values from -0.125 to 0.125
- down_pre: bfloat16 [5632, 2048], P('kv', 'tp'), may hold values from -0.078125 to 0.078125
- gain_mix: float32 [2048], replicated, may hold values from 0.1 to 1.9
- query_weight: bfloat16 [2048, 2048], P('kv', 'tp'), may hold values from -0.125 to 0.125
- forget_weight: bfloat16 [2048, 2048], P('kv', 'tp'), may hold values from -0.125 to 0.125
- value_weight: bfloat16 [2048, 2048], P('kv', 'tp'), may hold values from -0.125 to 0.125
- outgate_weight: bfloat16 [2048, 2048], P('kv', 'tp'), may hold values from -0.125 to 0.125
- lower_bound: float32 [2048], P('tp'), may hold values from 0.05 to 0.95
- head_gain: float32 [2048], P('tp'), may hold values from 0.1 to 1.9
- out_weight: bfloat16 [2048, 2048], P('tp'), may hold values from -0.125 to 0.125
- gain_post: float32 [2048], P('tp'), may hold values from 0.1 to 1.9
- gate_post: bfloat16 [2048, 5632], P('tp', 'kv'), may hold values from -0.125 to 0.125
- up_post: bfloat16 [2048, 5632], P('tp', 'kv'), may hold values from -0.125 to 0.125
- down_post: bfloat16 [5632, 2048], P('kv', 'tp'), may hold values from -0.078125 to 0.078125
- memory_state: float32 [96, 16, 128, 128], P('kv', 'tp'), may hold values from -4 to 4
Outputs:
- layer_out: bfloat16 [96, 2048], P('kv', 'tp')
- next_state: float32 [96, 16, 128, 128], P('kv', 'tp')
All inputs are finite; a program needn't handle non-finite values.
Results may differ from a plain program's by a relative error of at most 0.014.
Values may be sent and summed in bfloat16 or wider, within the bound.
A program may use at most 64 MiB of HBM per device.

v0:
```python
import jax
import jax.numpy as jnp
from jax import lax
from jax.sharding import PartitionSpec as P

D = 2048
HEAD_DIM = 128
EPSILON = 1e-06


def channel_mixer(row_block, gain_vec, gate_weight, up_weight, down_weight):
    gathered = lax.all_gather(row_block, "kv", axis=0, tiled=True)
    widened = gathered.astype(jnp.float32)
    part_squares = jnp.sum(widened * widened, axis=1)
    scaled = (widened * gain_vec).astype(jnp.bfloat16)
    gate_part = jnp.dot(scaled, gate_weight, preferred_element_type=jnp.float32)
    up_part = jnp.dot(scaled, up_weight, preferred_element_type=jnp.float32)
    gate_share, up_share, square_share = (
        lax.psum_scatter(
            gate_part.astype(jnp.bfloat16), "tp", scatter_dimension=0, tiled=True
        ).astype(jnp.float32),
        lax.psum_scatter(
            up_part.astype(jnp.bfloat16), "tp", scatter_dimension=0, tiled=True
        ).astype(jnp.float32),
        lax.psum_scatter(
            part_squares.astype(jnp.bfloat16), "tp", scatter_dimension=0, tiled=True
        ).astype(jnp.float32),
    )
    share_inverse = lax.rsqrt(square_share / D + EPSILON)[:, None]
    hidden_share = (jax.nn.silu(gate_share * share_inverse) * (up_share * share_inverse)).astype(
        jnp.bfloat16
    )
    hidden = lax.all_gather(hidden_share, "tp", axis=0, tiled=True)
    return lax.psum_scatter(
        jnp.dot(hidden, down_weight, preferred_element_type=jnp.float32),
        "kv",
        scatter_dimension=0,
        tiled=True,
    )


def token_mixer(
    stream_a,
    gain_mix,
    query_weight,
    forget_weight,
    value_weight,
    outgate_weight,
    lower_bound,
    head_gain,
    out_weight,
    memory_state,
):
    full_rows = lax.all_gather(stream_a, "tp", axis=1, tiled=True)
    widened = full_rows.astype(jnp.float32)
    inverse = lax.rsqrt(jnp.mean(widened * widened, axis=1, keepdims=True) + EPSILON)
    scaled = (widened * gain_mix).astype(jnp.bfloat16)
    weights = (query_weight, forget_weight, value_weight, outgate_weight)
    blocks = lax.all_to_all(scaled, "kv", split_axis=1, concat_axis=0, tiled=True)
    joined = jnp.concatenate(weights, axis=1)
    projected = lax.psum_scatter(
        jnp.dot(blocks, joined, preferred_element_type=jnp.float32),
        "kv",
        scatter_dimension=0,
        tiled=True,
    )
    projected = projected * inverse
    seq_rows = scaled.shape[0]
    local_heads = query_weight.shape[1] // HEAD_DIM
    reshaped = projected.reshape(seq_rows, 4, local_heads, HEAD_DIM)
    query_pre = reshaped[:, 0]
    forget_pre = reshaped[:, 1]
    value_pre = reshaped[:, 2]
    outgate_pre = reshaped[:, 3]
    floor_rate = lower_bound.reshape(local_heads, HEAD_DIM)
    log_keep = jnp.logaddexp(
        jnp.log(floor_rate), jnp.log1p(-floor_rate) + jax.nn.log_sigmoid(forget_pre)
    )
    inject = (1.0 - floor_rate) * jax.nn.sigmoid(-forget_pre)
    next_state = (
        jnp.exp(log_keep)[..., None] * memory_state + inject[..., None] * value_pre[:, :, None, :]
    )
    readout = jnp.einsum(
        "bhk,bhkv->bhv", jax.nn.silu(query_pre), next_state, precision=lax.Precision.HIGHEST
    )
    normed = (
        readout
        * lax.rsqrt(jnp.mean(readout * readout, axis=2, keepdims=True) + EPSILON)
        * head_gain.reshape(local_heads, HEAD_DIM)
    )
    mixed_heads = (
        (normed * jax.nn.silu(outgate_pre))
        .reshape(seq_rows, local_heads * HEAD_DIM)
        .astype(jnp.bfloat16)
    )
    partial_out = jnp.dot(mixed_heads, out_weight, preferred_element_type=jnp.float32)
    mixed = lax.psum_scatter(
        partial_out.astype(jnp.bfloat16), "tp", scatter_dimension=1, tiled=True
    ).astype(jnp.float32)
    return (mixed, next_state)


def shards(
    residual_in,
    gain_pre,
    gate_pre,
    up_pre,
    down_pre,
    gain_mix,
    query_weight,
    forget_weight,
    value_weight,
    outgate_weight,
    lower_bound,
    head_gain,
    out_weight,
    gain_post,
    gate_post,
    up_post,
    down_post,
    memory_state,
):
    branch_a = channel_mixer(residual_in, gain_pre, gate_pre, up_pre, down_pre)
    stream_a = (residual_in.astype(jnp.float32) + 0.5 * branch_a).astype(jnp.bfloat16)
    mixed, next_state = token_mixer(
        stream_a,
        gain_mix,
        query_weight,
        forget_weight,
        value_weight,
        outgate_weight,
        lower_bound,
        head_gain,
        out_weight,
        memory_state,
    )
    stream_b = (stream_a.astype(jnp.float32) + mixed).astype(jnp.bfloat16)
    branch_b = channel_mixer(stream_b, gain_post, gate_post, up_post, down_post)
    layer_out = (stream_b.astype(jnp.float32) + 0.5 * branch_b).astype(jnp.bfloat16)
    return (layer_out, next_state)


def solution(mesh):
    in_specs = (
        P("kv", "tp"),
        P("tp"),
        P("tp", "kv"),
        P("tp", "kv"),
        P("kv", "tp"),
        P(),
        P("kv", "tp"),
        P("kv", "tp"),
        P("kv", "tp"),
        P("kv", "tp"),
        P("tp"),
        P("tp"),
        P("tp", None),
        P("tp"),
        P("tp", "kv"),
        P("tp", "kv"),
        P("kv", "tp"),
        P("kv", "tp", None, None),
    )
    out_specs = (P("kv", "tp"), P("kv", "tp", None, None))
    return jax.shard_map(shards, mesh=mesh, in_specs=in_specs, out_specs=out_specs, check_vma=False)
```

profile of v0, /device:TPU:18, one launch (start us, length us, event | category | flops | bytes accessed | tf_op | source)
XLA Modules:
  0.0 353.3 jit_solution(17581845288127005112)
XLA Ops:
  7.3 30.5 %all-gather = bf16[16,6,1024]{2,1,0:T(8,128)(2,1)S(1)} all-gather(bf16[1,6,1024]{2,1,0:T(8,128)(2,1)} %bitcast.90), channel_id=1, replica_groups=mesh['kv'=16,'tp'=2] {'kv'}, dimensions={0}, use_global_device_ids=true | all-gather | bytes 208896 | tf_op jit(solution)/shard_map/all_gather | solution.py:12
  37.9 2.2 convolution_convert_fusion.4
  40.2 2.1 convolution_convert_fusion.3
  42.4 0.6 dynamic-slice
  43.7 2.5 all-reduce
  46.2 9.6 %reduce-scatter.12.cloned.1.call-done = bf16[48,352]{1,0:T(8,128)(2,1)} async-done(((bf16[96,352]{1,0:T(8,128)(2,1)}), bf16[48,352]{1,0:T(8,128)(2,1)}) %reduce-scatter.12.cloned.1.call-update) | async-done | bytes 33808 | tf_op jit(solution)/shard_map/reduce_scatter | solution.py:19
  55.8 11.4 %reduce-scatter.14.cloned.1.call-done = bf16[48,352]{1,0:T(8,128)(2,1)} async-done(((bf16[96,352]{1,0:T(8,128)(2,1)}), bf16[48,352]{1,0:T(8,128)(2,1)}) %reduce-scatter.14.cloned.1.call-update) | async-done | bytes 33808 | tf_op jit(solution)/shard_map/reduce_scatter | solution.py:22
  67.3 0.9 multiply_convert_fusion.3
  68.2 1.9 all_gather.16
  70.3 35.6 %fusion = f32[8,1024]{1,0:T(8,128)S(1)} fusion(f32[96,1024]{1,0:T(8,128)S(1)} %fusion.36), kind=kCustom, calls=%all-reduce-scatter | all-reduce-scatter fusion | flops 131073 | bytes 426496
  105.9 6.0 %collective-permute-start.2 = (f32[8,1024]{1,0:T(8,128)S(1)}, f32[8,1024]{1,0:T(8,128)S(1)}, u32[]{:S(2)}, u32[]{:S(2)}) collective-permute-start(f32[8,1024]{1,0:T(8,128)S(1)} %fusion), channel_id=1, source_target_pairs={{0,6},{2,8},{4,10},{6,12},{8,14},{10,16},{12,18},{14,20},{16,22},{... | collective-permute-start | bytes 98312
  111.9 4.4 %collective-permute-start.1 = (f32[8,1024]{1,0:T(8,128)S(1)}, f32[8,1024]{1,0:T(8,128)S(1)}, u32[]{:S(2)}, u32[]{:S(2)}) collective-permute-start(f32[8,1024]{1,0:T(8,128)S(1)} %fusion), channel_id=1, source_target_pairs={{0,4},{2,6},{4,8},{6,10},{8,12},{10,14},{12,16},{14,18},{16,20},{1... | collective-permute-start | bytes 98312
  116.3 4.9 %collective-permute-start = (f32[8,1024]{1,0:T(8,128)S(1)}, f32[8,1024]{1,0:T(8,128)S(1)}, u32[]{:S(2)}, u32[]{:S(2)}) collective-permute-start(f32[8,1024]{1,0:T(8,128)S(1)} %fusion), channel_id=1, source_target_pairs={{0,2},{2,4},{4,6},{6,8},{8,10},{10,12},{12,14},{14,16},{16,18},{18... | collective-permute-start | bytes 98312
  121.2 1.9 collective-permute-start.3
  123.1 0.6 dynamic-slice.12
  124.4 2.6 collective-permute-done.3
  127.5 1.8 all_gather.17
  129.3 0.7 fusion.13
  130.1 5.1 %all-to-all-start = ((bf16[6,16,128]{2,0,1:T(8,128)(2,1)}), bf16[6,16,128]{2,0,1:T(8,128)(2,1)S(1)}, u32[]{:S(2)}, u32[]{:S(2)}) async-start(bf16[6,16,128]{2,0,1:T(8,128)(2,1)} %get-tuple-element.6), calls=%async_computation.2 | async-start | bytes 65536 | tf_op jit(solution)/shard_map/all_to_all | solution.py:59
  135.3 4.3 %all-to-all-done = bf16[6,16,128]{2,0,1:T(8,128)(2,1)S(1)} async-done(((bf16[6,16,128]{2,0,1:T(8,128)(2,1)}), bf16[6,16,128]{2,0,1:T(8,128)(2,1)S(1)}, u32[]{:S(2)}, u32[]{:S(2)}) %all-to-all-start) | async-done | bytes 24608 | tf_op jit(solution)/shard_map/all_to_all | solution.py:59
  139.9 52.3 %fusion.1 = f32[8,4096]{1,0:T(8,128)S(1)} fusion(f32[96,4096]{1,0:T(8,128)S(1)} %fusion.3), kind=kCustom, calls=%all-reduce-scatter.1 | all-reduce-scatter fusion | flops 524289 | bytes 1704448
  192.3 3.3 collective-permute-start.6
  195.5 3.0 collective-permute-start.5
  198.5 3.5 collective-permute-start.4
  202.0 1.9 collective-permute-start.7
  204.0 4.9 %collective-permute-done.7 = f32[6,4096]{1,0:T(8,128)S(1)} collective-permute-done((f32[6,4096]{1,0:T(8,128)S(1)}, f32[6,4096]{1,0:T(8,128)S(1)}, u32[]{:S(2)}, u32[]{:S(2)}) %collective-permute-start.7) | collective-permute-done | bytes 98336
  208.9 0.8 concatenate.5
  209.9 4.0 %multiply_add_fusion = f32[6,8,128,128]{3,2,1,0:T(8,128)S(1)} fusion(f32[6,8,128,128]{3,2,1,0:T(8,128)} %param.35, f32[6,8,128]{2,1,0:T(8,128)S(1)} %slice_bitcast_fusion.1, f32[6,8,128]{2,1,0:T(8,128)S(1)} %get-tuple-element.3, f32[6,8,128]{2,1,0:T(8,128)S(1)} %get-tuple-element.2), kind=kLoop, calls=%fused_computation | loop fusion | flops 2359296 | bytes 6365184 | tf_op jit(solution)/shard_map/add | solution.py:81
  213.9 1.6 copy-done.1
  215.6 2.8 fusion.37
  218.5 1.3 convolution_convert_fusion
  219.9 7.1 %reduce-scatter.16.cloned.1.call-done = bf16[6,1024]{1,0:T(8,128)(2,1)} async-done(((bf16[6,2048]{1,0:T(8,128)(2,1)}), bf16[6,1024]{1,0:T(8,128)(2,1)}) %reduce-scatter.16.cloned.1.call-update) | async-done | bytes 12304 | tf_op jit(solution)/shard_map/reduce_scatter | solution.py:97
  226.9 0.7 fusion.28
  227.7 30.4 %all-gather.1 = bf16[16,6,1024]{2,1,0:T(8,128)(2,1)S(1)} all-gather(bf16[1,6,1024]{2,1,0:T(8,128)(2,1)S(1)} %fusion.28), channel_id=1, replica_groups=mesh['kv'=16,'tp'=2] {'kv'}, dimensions={0}, use_global_device_ids=true | all-gather | bytes 208896 | tf_op jit(solution)/shard_map/all_gather | solution.py:12
  258.1 1.7 convolution_convert_fusion.2
  259.9 1.7 convolution_convert_fusion.1
  261.7 2.5 all-reduce.3
  264.3 11.0 %reduce-scatter.18.cloned.1.call-done = bf16[48,352]{1,0:T(8,128)(2,1)} async-done(((bf16[96,352]{1,0:T(8,128)(2,1)}), bf16[48,352]{1,0:T(8,128)(2,1)}) %reduce-scatter.18.cloned.1.call-update) | async-done | bytes 33808 | tf_op jit(solution)/shard_map/reduce_scatter | solution.py:19
  275.3 10.7 %reduce-scatter.20.cloned.1.call-done = bf16[48,352]{1,0:T(8,128)(2,1)} async-done(((bf16[96,352]{1,0:T(8,128)(2,1)}), bf16[48,352]{1,0:T(8,128)(2,1)}) %reduce-scatter.20.cloned.1.call-update) | async-done | bytes 33808 | tf_op jit(solution)/shard_map/reduce_scatter | solution.py:22
  286.0 0.9 multiply_convert_fusion.2
  286.9 1.9 all_gather.19
  289.1 35.5 %fusion.2 = f32[8,1024]{1,0:T(8,128)S(1)} fusion(f32[96,1024]{1,0:T(8,128)S(1)} %fusion.38), kind=kCustom, calls=%all-reduce-scatter.2 | all-reduce-scatter fusion | flops 131073 | bytes 426496
  324.6 6.1 %collective-permute-start.10 = (f32[8,1024]{1,0:T(8,128)S(1)}, f32[8,1024]{1,0:T(8,128)S(1)}, u32[]{:S(2)}, u32[]{:S(2)}) collective-permute-start(f32[8,1024]{1,0:T(8,128)S(1)} %fusion.2), channel_id=1, source_target_pairs={{0,6},{2,8},{4,10},{6,12},{8,14},{10,16},{12,18},{14,20},{16,22},{... | collective-permute-start | bytes 98312
  330.6 4.4 %collective-permute-start.9 = (f32[8,1024]{1,0:T(8,128)S(1)}, f32[8,1024]{1,0:T(8,128)S(1)}, u32[]{:S(2)}, u32[]{:S(2)}) collective-permute-start(f32[8,1024]{1,0:T(8,128)S(1)} %fusion.2), channel_id=1, source_target_pairs={{0,4},{2,6},{4,8},{6,10},{8,12},{10,14},{12,16},{14,18},{16,20},{1... | collective-permute-start | bytes 98312
  335.0 4.9 %collective-permute-start.8 = (f32[8,1024]{1,0:T(8,128)S(1)}, f32[8,1024]{1,0:T(8,128)S(1)}, u32[]{:S(2)}, u32[]{:S(2)}) collective-permute-start(f32[8,1024]{1,0:T(8,128)S(1)} %fusion.2), channel_id=1, source_target_pairs={{0,2},{2,4},{4,6},{6,8},{8,10},{10,12},{12,14},{14,16},{16,18},{18... | collective-permute-start | bytes 98312
  339.9 1.9 collective-permute-start.11
  341.8 3.9 %collective-permute-done.11 = f32[6,1024]{1,0:T(8,128)S(1)} collective-permute-done((f32[6,1024]{1,0:T(8,128)S(1)}, f32[6,1024]{1,0:T(8,128)S(1)}, u32[]{:S(2)}, u32[]{:S(2)}) %collective-permute-start.11) | collective-permute-done | bytes 24608
  346.2 0.6 fusion.16
  (77 shorter events, 3.1 us)
Async XLA Ops:
  7.2 62.9 %copy-start = (bf16[352,1024]{1,0:T(8,128)(2,1)S(1)}, bf16[352,1024]{1,0:T(8,128)(2,1)}, u32[]{:S(2)}) copy-start(bf16[352,1024]{1,0:T(8,128)(2,1)} %param.22) | copy-start | bytes 2162692
  7.2 35.2 %copy-start.16 = (u32[32]{0:T(128)S(1)}, u32[32]{0:T(128)}, u32[]{:S(2)}) copy-start(u32[32]{0:T(128)} %constant.33) | copy-start | bytes 388
  7.2 115.9 %copy-start.11 = (u32[32]{0:T(128)S(1)}, u32[32]{0:T(128)}, u32[]{:S(2)}) copy-start(u32[32]{0:T(128)} %constant.37) | copy-start | bytes 388
  7.2 120.3 %copy-start.6 = (bf16[6,1024]{1,0:T(8,128)(2,1)S(1)}, bf16[6,1024]{1,0:T(8,128)(2,1)}, u32[]{:S(2)}) copy-start(bf16[6,1024]{1,0:T(8,128)(2,1)} %param.18) | copy-start | bytes 36868
  7.2 122.1 %copy-start.8 = (f32[2048]{0:T(1024)S(1)}, f32[2048]{0:T(1024)}, u32[]{:S(2)}) copy-start(f32[2048]{0:T(1024)} %param.23) | copy-start | bytes 24580
  7.2 48.6 %reduce-scatter.12.cloned.1.call-start = ((), (), s32[]{:S(2)}) async-start(), calls=%async_computation.6 | async-start | bytes 110592 | tf_op jit(solution)/shard_map/reduce_scatter | solution.py:19
  7.3 128.0 %copy-start.10 = (f32[1024]{0:T(1024)S(1)}, f32[1024]{0:T(1024)}, u32[]{:S(2)}) copy-start(f32[1024]{0:T(1024)} %param.28) | copy-start | bytes 12292
  37.8 101.7 %copy-start.12 = (bf16[128,1024]{1,0:T(8,128)(2,1)S(1)}, bf16[128,1024]{1,0:T(8,128)(2,1)}, u32[]{:S(2)}) copy-start(bf16[128,1024]{1,0:T(8,128)(2,1)} %param.27) | copy-start | bytes 786436
  37.8 101.7 %copy-start.13 = (bf16[128,1024]{1,0:T(8,128)(2,1)S(1)}, bf16[128,1024]{1,0:T(8,128)(2,1)}, u32[]{:S(2)}) copy-start(bf16[128,1024]{1,0:T(8,128)(2,1)} %param.26) | copy-start | bytes 786436
  37.8 101.7 %copy-start.14 = (bf16[128,1024]{1,0:T(8,128)(2,1)S(1)}, bf16[128,1024]{1,0:T(8,128)(2,1)}, u32[]{:S(2)}) copy-start(bf16[128,1024]{1,0:T(8,128)(2,1)} %param.25) | copy-start | bytes 786436
  37.8 101.7 %copy-start.15 = (bf16[128,1024]{1,0:T(8,128)(2,1)S(1)}, bf16[128,1024]{1,0:T(8,128)(2,1)}, u32[]{:S(2)}) copy-start(bf16[128,1024]{1,0:T(8,128)(2,1)} %param.24) | copy-start | bytes 786436
  40.1 27.2 %reduce-scatter.14.cloned.1.call-start = ((), (), s32[]{:S(2)}) async-start(), calls=%async_computation.7 | async-start | bytes 110592 | tf_op jit(solution)/shard_map/reduce_scatter | solution.py:22
  105.9 21.1 %collective-permute-start.2 = (f32[8,1024]{1,0:T(8,128)S(1)}, f32[8,1024]{1,0:T(8,128)S(1)}, u32[]{:S(2)}, u32[]{:S(2)}) collective-permute-start(f32[8,1024]{1,0:T(8,128)S(1)} %fusion), channel_id=1, source_target_pairs={{0,6},{2,8},{4,10},{6,12},{8,14},{10,16},{12,18},{14,20},{16,22},{... | collective-permute-start | bytes 98312
  111.9 15.1 %collective-permute-start.1 = (f32[8,1024]{1,0:T(8,128)S(1)}, f32[8,1024]{1,0:T(8,128)S(1)}, u32[]{:S(2)}, u32[]{:S(2)}) collective-permute-start(f32[8,1024]{1,0:T(8,128)S(1)} %fusion), channel_id=1, source_target_pairs={{0,4},{2,6},{4,8},{6,10},{8,12},{10,14},{12,16},{14,18},{16,20},{1... | collective-permute-start | bytes 98312
  116.3 10.7 %collective-permute-start = (f32[8,1024]{1,0:T(8,128)S(1)}, f32[8,1024]{1,0:T(8,128)S(1)}, u32[]{:S(2)}, u32[]{:S(2)}) collective-permute-start(f32[8,1024]{1,0:T(8,128)S(1)} %fusion), channel_id=1, source_target_pairs={{0,2},{2,4},{4,6},{6,8},{8,10},{10,12},{12,14},{14,16},{16,18},{18... | collective-permute-start | bytes 98312
  121.2 5.8 %collective-permute-start.3 = (f32[6,1024]{1,0:T(8,128)S(1)}, f32[6,1024]{1,0:T(8,128)S(1)}, u32[]{:S(2)}, u32[]{:S(2)}) collective-permute-start(f32[6,1024]{1,0:T(8,128)S(1)} %slice.20), channel_id=1, source_target_pairs={{0,8},{2,10},{4,12},{6,14},{8,16},{10,18},{12,20},{14,22},{16,24},... | collective-permute-start | bytes 73736
  130.1 9.4 %all-to-all-start = ((bf16[6,16,128]{2,0,1:T(8,128)(2,1)}), bf16[6,16,128]{2,0,1:T(8,128)(2,1)S(1)}, u32[]{:S(2)}, u32[]{:S(2)}) async-start(bf16[6,16,128]{2,0,1:T(8,128)(2,1)} %get-tuple-element.6), calls=%async_computation.2 | async-start | bytes 65536 | tf_op jit(solution)/shard_map/all_to_all | solution.py:59
  135.2 91.8 %reduce-scatter.16.cloned.1.call-start = ((), (), s32[]{:S(2)}) async-start(), calls=%async_computation.8 | async-start | bytes 49152 | tf_op jit(solution)/shard_map/reduce_scatter | solution.py:97
  192.3 16.6 %collective-permute-start.6 = (f32[8,4096]{1,0:T(8,128)S(1)}, f32[8,4096]{1,0:T(8,128)S(1)}, u32[]{:S(2)}, u32[]{:S(2)}) collective-permute-start(f32[8,4096]{1,0:T(8,128)S(1)} %fusion.1), channel_id=1, source_target_pairs={{0,6},{2,8},{4,10},{6,12},{8,14},{10,16},{12,18},{14,20},{16,22},{... | collective-permute-start | bytes 393224
  195.5 13.4 %collective-permute-start.5 = (f32[8,4096]{1,0:T(8,128)S(1)}, f32[8,4096]{1,0:T(8,128)S(1)}, u32[]{:S(2)}, u32[]{:S(2)}) collective-permute-start(f32[8,4096]{1,0:T(8,128)S(1)} %fusion.1), channel_id=1, source_target_pairs={{0,4},{2,6},{4,8},{6,10},{8,12},{10,14},{12,16},{14,18},{16,20},{1... | collective-permute-start | bytes 393224
  198.5 10.4 %collective-permute-start.4 = (f32[8,4096]{1,0:T(8,128)S(1)}, f32[8,4096]{1,0:T(8,128)S(1)}, u32[]{:S(2)}, u32[]{:S(2)}) collective-permute-start(f32[8,4096]{1,0:T(8,128)S(1)} %fusion.1), channel_id=1, source_target_pairs={{0,2},{2,4},{4,6},{6,8},{8,10},{10,12},{12,14},{14,16},{16,18},{18... | collective-permute-start | bytes 393224
  202.0 6.9 %collective-permute-start.7 = (f32[6,4096]{1,0:T(8,128)S(1)}, f32[6,4096]{1,0:T(8,128)S(1)}, u32[]{:S(2)}, u32[]{:S(2)}) collective-permute-start(f32[6,4096]{1,0:T(8,128)S(1)} %slice.21), channel_id=1, source_target_pairs={{0,8},{2,10},{4,12},{6,14},{8,16},{10,18},{12,20},{14,22},{16,24},... | collective-permute-start | bytes 294920
  209.9 8.6 %copy-start.2 = (bf16[1024,2048]{1,0:T(8,128)(2,1)S(1)}, bf16[1024,2048]{1,0:T(8,128)(2,1)}, u32[]{:S(2)}) copy-start(bf16[1024,2048]{1,0:T(8,128)(2,1)} %param.30) | copy-start | bytes 12582916
  213.9 1.7 copy-start.1
  213.9 4.5 %copy-start.9 = (f32[1024]{0:T(1024)S(1)}, f32[1024]{0:T(1024)}, u32[]{:S(2)}) copy-start(f32[1024]{0:T(1024)} %param.29) | copy-start | bytes 12292
  218.3 39.8 %copy-start.3 = (bf16[1024,352]{0,1:T(8,128)(2,1)S(1)}, bf16[1024,352]{0,1:T(8,128)(2,1)}, u32[]{:S(2)}) copy-start(bf16[1024,352]{0,1:T(8,128)(2,1)} %param.32) | copy-start | bytes 2162692
  218.5 41.4 %copy-start.4 = (bf16[1024,352]{0,1:T(8,128)(2,1)S(1)}, bf16[1024,352]{0,1:T(8,128)(2,1)}, u32[]{:S(2)}) copy-start(bf16[1024,352]{0,1:T(8,128)(2,1)} %param.33) | copy-start | bytes 2162692
  219.8 69.0 %copy-start.5 = (bf16[352,1024]{1,0:T(8,128)(2,1)S(1)}, bf16[352,1024]{1,0:T(8,128)(2,1)}, u32[]{:S(2)}) copy-start(bf16[352,1024]{1,0:T(8,128)(2,1)} %param.34) | copy-start | bytes 2162692
  219.8 55.5 %reduce-scatter.18.cloned.1.call-start = ((), (), s32[]{:S(2)}) async-start(), calls=%async_computation.9 | async-start | bytes 110592 | tf_op jit(solution)/shard_map/reduce_scatter | solution.py:19
  258.1 88.0 %copy-start.7 = (bf16[6,1024]{1,0:T(8,128)(2,1)S(1)}, bf16[6,1024]{1,0:T(8,128)(2,1)}, u32[]{:S(2)}) copy-start(bf16[6,1024]{1,0:T(8,128)(2,1)} %reduce-scatter.16.cloned.1.call-done) | copy-start | bytes 36868
  259.8 26.2 %reduce-scatter.20.cloned.1.call-start = ((), (), s32[]{:S(2)}) async-start(), calls=%async_computation.10 | async-start | bytes 110592 | tf_op jit(solution)/shard_map/reduce_scatter | solution.py:22
  324.6 21.1 %collective-permute-start.10 = (f32[8,1024]{1,0:T(8,128)S(1)}, f32[8,1024]{1,0:T(8,128)S(1)}, u32[]{:S(2)}, u32[]{:S(2)}) collective-permute-start(f32[8,1024]{1,0:T(8,128)S(1)} %fusion.2), channel_id=1, source_target_pairs={{0,6},{2,8},{4,10},{6,12},{8,14},{10,16},{12,18},{14,20},{16,22},{... | collective-permute-start | bytes 98312
  330.6 15.1 %collective-permute-start.9 = (f32[8,1024]{1,0:T(8,128)S(1)}, f32[8,1024]{1,0:T(8,128)S(1)}, u32[]{:S(2)}, u32[]{:S(2)}) collective-permute-start(f32[8,1024]{1,0:T(8,128)S(1)} %fusion.2), channel_id=1, source_target_pairs={{0,4},{2,6},{4,8},{6,10},{8,12},{10,14},{12,16},{14,18},{16,20},{1... | collective-permute-start | bytes 98312
  335.0 10.7 %collective-permute-start.8 = (f32[8,1024]{1,0:T(8,128)S(1)}, f32[8,1024]{1,0:T(8,128)S(1)}, u32[]{:S(2)}, u32[]{:S(2)}) collective-permute-start(f32[8,1024]{1,0:T(8,128)S(1)} %fusion.2), channel_id=1, source_target_pairs={{0,2},{2,4},{4,6},{6,8},{8,10},{10,12},{12,14},{14,16},{16,18},{18... | collective-permute-start | bytes 98312
  339.9 5.8 %collective-permute-start.11 = (f32[6,1024]{1,0:T(8,128)S(1)}, f32[6,1024]{1,0:T(8,128)S(1)}, u32[]{:S(2)}, u32[]{:S(2)}) collective-permute-start(f32[6,1024]{1,0:T(8,128)S(1)} %slice.22), channel_id=1, source_target_pairs={{0,8},{2,10},{4,12},{6,14},{8,16},{10,18},{12,20},{14,22},{16,24},... | collective-permute-start | bytes 73736
Sparse Core Ops, SparseCore 0:
  40.2 15.5 reduce-scatter.11
  58.6 8.6 reduce-scatter.13
  219.9 6.9 reduce-scatter.15
  260.0 15.2 reduce-scatter.17
  277.3 8.6 reduce-scatter.19
where the time goes:
time: 354 us; the launch traced here: 353 us
  blocking collectives  195 us (55%)
  waiting for transfers between devices  65.7 us (19%)
  starting transfers between devices  51.3 us (14%)
  between operations  15.6 us (4%)
  matrix products  12.6 us (4%)
  other arithmetic  8.58 us (2%)
  local copies, waits for them, and re-layouts  4.76 us (1%)
    unnamed x5, blocking collectives  128 us
    all_gather x2, blocking collectives, channel_mixer(): gathered = lax.all_gather(row_block, 'kv', axis=0, tiled=True)  60.9 us
    unnamed x12, starting transfers between devices  46 us
    reduce_scatter x2, waiting for transfers between devices, channel_mixer(): lax.psum_scatter(up_part.astype(jnp.bfloat16), 'tp', scatter_dimension=0,...  22.2 us
    reduce_scatter x2, waiting for transfers between devices, channel_mixer(): lax.psum_scatter(gate_part.astype(jnp.bfloat16), 'tp', scatter_dimension=...  20.7 us
    unnamed x17, waiting for transfers between devices  11.5 us
  transfers between devices with their start and end apart: 18, of which 9 were waited for; matrix products, arithmetic and copies ran while one was open for 2% of the time, Pallas kernels for 0%

commit v1 on v0

--- a/solution.py
+++ b/solution.py
@@ -8,8 +8,18 @@
 EPSILON = 1e-06
 
 
+def turned_line(x, axis, along):
+    peers = lax.axis_size(axis)
+    held, parts = (x, [x])
+    for _ in range(peers - 1):
+        held = lax.ppermute(held, axis, [(i, (i + 1) % peers) for i in range(peers)])
+        parts.insert(0, held)
+    line = jnp.concatenate(parts, axis=along)
+    return jnp.roll(line, (lax.axis_index(axis) + 1) * x.shape[along], axis=along)
+
+
 def channel_mixer(row_block, gain_vec, gate_weight, up_weight, down_weight):
-    gathered = lax.all_gather(row_block, "kv", axis=0, tiled=True)
+    gathered = turned_line(row_block, "kv", 0)
     widened = gathered.astype(jnp.float32)
     part_squares = jnp.sum(widened * widened, axis=1)
     scaled = (widened * gain_vec).astype(jnp.bfloat16)

time: 354 us -> 493 us (1.39)
  waiting for transfers between devices: 65.7 us -> 237 us
  blocking collectives: 195 us -> 134 us
  starting transfers between devices: 51.3 us -> 76.9 us
    ppermute x0 -> x30, waiting for transfers between devices: none -> 134 us  [turned_line(): lax.ppermute(held, axis, [(i, (i + 1) % peers) for i in range(peers)])]
    all_gather x2 -> x0, blocking collectives: 60.9 us -> none  [channel_mixer(): gathered = lax.all_gather(row_block, 'kv', axis=0, tiled=True)]
    reduce_scatter x2, waiting for transfers between devices: 20.7 us -> 57.3 us  [channel_mixer(): lax.psum_scatter(gate_part.astype(jnp.bfloat16), 'tp', scatter_dimension=...]
    ppermute x0 -> x30, starting transfers between devices: none -> 25.6 us  [turned_line(): lax.ppermute(held, axis, [(i, (i + 1) % peers) for i in range(peers)])]
  transfers between devices with their start and end apart: 18 -> 48, of which waited for: 9 -> 39; matrix products, arithmetic and copies ran while one was open for 2% -> 1% of each run, Pallas kernels for 0% -> 0%
where the time goes in v1:
time: 493 us; the launch traced here: 492 us
  waiting for transfers between devices  237 us (48%)
  blocking collectives  134 us (27%)
  starting transfers between devices  76.9 us (16%)
  between operations  15.6 us (3%)
  matrix products  12.2 us (2%)
  other arithmetic  8.88 us (2%)
  local copies, waits for them, and re-layouts  7.96 us (2%)
    ppermute x30, waiting for transfers between devices, turned_line(): lax.ppermute(held, axis, [(i, (i + 1) % peers) for i in range(peers)])  134 us
    unnamed x5, blocking collectives  128 us
    reduce_scatter x2, waiting for transfers between devices, channel_mixer(): lax.psum_scatter(gate_part.astype(jnp.bfloat16), 'tp', scatter_dimension=...  57.3 us
    unnamed x12, starting transfers between devices  45.9 us
    ppermute x30, starting transfers between devices, turned_line(): lax.ppermute(held, axis, [(i, (i + 1) % peers) for i in range(peers)])  25.6 us
    reduce_scatter x2, waiting for transfers between devices, channel_mixer(): lax.psum_scatter(up_part.astype(jnp.bfloat16), 'tp', scatter_dimension=0,...  22.2 us
    unnamed x17, waiting for transfers between devices  11.5 us
  transfers between devices with their start and end apart: 48, of which 39 were waited for; matrix products, arithmetic and copies ran while one was open for 1% of the time, Pallas kernels for 0%

profile of v1, /device:TPU:18, one launch (start us, length us, event | category | flops | bytes accessed | tf_op | source)
XLA Modules:
  0.0 492.1 jit_solution(15458967305459657561)
XLA Ops:
  15.3 3.0 collective-permute-start.2
  23.1 3.4 collective-permute-done.3
  27.7 4.2 collective-permute-done.4
  32.4 5.1 %collective-permute-done.5 = bf16[6,1024]{1,0:T(8,128)(2,1)S(1)} collective-permute-done((bf16[6,1024]{1,0:T(8,128)(2,1)S(1)}, bf16[6,1024]{1,0:T(8,128)(2,1)S(1)}, u32[]{:S(2)}, u32[]{:S(2)}) %collective-permute-start.5) | collective-permute-done | bytes 12320 | tf_op jit(solution)/shard_map/ppermute | solution.py:15
  37.5 5.5 %collective-permute-done.6 = bf16[6,1024]{1,0:T(8,128)(2,1)S(1)} collective-permute-done((bf16[6,1024]{1,0:T(8,128)(2,1)S(1)}, bf16[6,1024]{1,0:T(8,128)(2,1)S(1)}, u32[]{:S(2)}, u32[]{:S(2)}) %collective-permute-start.6) | collective-permute-done | bytes 12320 | tf_op jit(solution)/shard_map/ppermute | solution.py:15
  43.0 5.6 %collective-permute-done.7 = bf16[6,1024]{1,0:T(8,128)(2,1)S(1)} collective-permute-done((bf16[6,1024]{1,0:T(8,128)(2,1)S(1)}, bf16[6,1024]{1,0:T(8,128)(2,1)S(1)}, u32[]{:S(2)}, u32[]{:S(2)}) %collective-permute-start.7) | collective-permute-done | bytes 12320 | tf_op jit(solution)/shard_map/ppermute | solution.py:15
  48.6 5.5 %collective-permute-done.8 = bf16[6,1024]{1,0:T(8,128)(2,1)S(1)} collective-permute-done((bf16[6,1024]{1,0:T(8,128)(2,1)S(1)}, bf16[6,1024]{1,0:T(8,128)(2,1)S(1)}, u32[]{:S(2)}, u32[]{:S(2)}) %collective-permute-start.8) | collective-permute-done | bytes 12320 | tf_op jit(solution)/shard_map/ppermute | solution.py:15
  54.1 5.5 %collective-permute-done.9 = bf16[6,1024]{1,0:T(8,128)(2,1)S(1)} collective-permute-done((bf16[6,1024]{1,0:T(8,128)(2,1)S(1)}, bf16[6,1024]{1,0:T(8,128)(2,1)S(1)}, u32[]{:S(2)}, u32[]{:S(2)}) %collective-permute-start.9) | collective-permute-done | bytes 12320 | tf_op jit(solution)/shard_map/ppermute | solution.py:15
  59.6 5.5 %collective-permute-done.10 = bf16[6,1024]{1,0:T(8,128)(2,1)S(1)} collective-permute-done((bf16[6,1024]{1,0:T(8,128)(2,1)S(1)}, bf16[6,1024]{1,0:T(8,128)(2,1)S(1)}, u32[]{:S(2)}, u32[]{:S(2)}) %collective-permute-start.10) | collective-permute-done | bytes 12320 | tf_op jit(solution)/shard_map/ppermute | solution.py:15
  65.2 5.5 %collective-permute-done.11 = bf16[6,1024]{1,0:T(8,128)(2,1)S(1)} collective-permute-done((bf16[6,1024]{1,0:T(8,128)(2,1)S(1)}, bf16[6,1024]{1,0:T(8,128)(2,1)S(1)}, u32[]{:S(2)}, u32[]{:S(2)}) %collective-permute-start.11) | collective-permute-done | bytes 12320 | tf_op jit(solution)/shard_map/ppermute | solution.py:15
  70.7 5.5 %collective-permute-done.12 = bf16[6,1024]{1,0:T(8,128)(2,1)S(1)} collective-permute-done((bf16[6,1024]{1,0:T(8,128)(2,1)S(1)}, bf16[6,1024]{1,0:T(8,128)(2,1)S(1)}, u32[]{:S(2)}, u32[]{:S(2)}) %collective-permute-start.12) | collective-permute-done | bytes 12320 | tf_op jit(solution)/shard_map/ppermute | solution.py:15
  76.5 5.3 %collective-permute-done.13 = bf16[6,1024]{1,0:T(8,128)(2,1)S(1)} collective-permute-done((bf16[6,1024]{1,0:T(8,128)(2,1)S(1)}, bf16[6,1024]{1,0:T(8,128)(2,1)S(1)}, u32[]{:S(2)}, u32[]{:S(2)}) %collective-permute-start.13) | collective-permute-done | bytes 12320 | tf_op jit(solution)/shard_map/ppermute | solution.py:15
  83.9 3.5 collective-permute-done.14
  98.1 27.2 %reduce-scatter.12.cloned.1.call-done = bf16[48,352]{1,0:T(8,128)(2,1)} async-done(((bf16[96,352]{1,0:T(8,128)(2,1)}), bf16[48,352]{1,0:T(8,128)(2,1)}) %reduce-scatter.12.cloned.1.call-update) | async-done | bytes 33808 | tf_op jit(solution)/shard_map/reduce_scatter | solution.py:29
  125.3 11.5 %reduce-scatter.14.cloned.1.call-done = bf16[48,352]{1,0:T(8,128)(2,1)} async-done(((bf16[96,352]{1,0:T(8,128)(2,1)}), bf16[48,352]{1,0:T(8,128)(2,1)}) %reduce-scatter.14.cloned.1.call-update) | async-done | bytes 33808 | tf_op jit(solution)/shard_map/reduce_scatter | solution.py:32
  139.8 35.6 %fusion = f32[8,1024]{1,0:T(8,128)S(1)} fusion(f32[96,1024]{1,0:T(8,128)S(1)} %fusion.47), kind=kCustom, calls=%all-reduce-scatter | all-reduce-scatter fusion | flops 131073 | bytes 426496
  175.4 6.0 %collective-permute-start.32 = (f32[8,1024]{1,0:T(8,128)S(1)}, f32[8,1024]{1,0:T(8,128)S(1)}, u32[]{:S(2)}, u32[]{:S(2)}) collective-permute-start(f32[8,1024]{1,0:T(8,128)S(1)} %fusion), channel_id=1, source_target_pairs={{0,6},{2,8},{4,10},{6,12},{8,14},{10,16},{12,18},{14,20},{16,22},{... | collective-permute-start | bytes 98312
  181.4 4.3 collective-permute-start.31
  185.8 4.9 collective-permute-start.30
  199.5 5.1 %all-to-all-start = ((bf16[6,16,128]{2,0,1:T(8,128)(2,1)}), bf16[6,16,128]{2,0,1:T(8,128)(2,1)S(1)}, u32[]{:S(2)}, u32[]{:S(2)}) async-start(bf16[6,16,128]{2,0,1:T(8,128)(2,1)} %get-tuple-element.11), calls=%async_computation.2 | async-start | bytes 65536 | tf_op jit(solution)/shard_map/all_to_all | solution.py:69
  204.7 4.3 all-to-all-done
  210.4 52.3 %fusion.1 = f32[8,4096]{1,0:T(8,128)S(1)} fusion(f32[96,4096]{1,0:T(8,128)S(1)} %fusion.3), kind=kCustom, calls=%all-reduce-scatter.1 | all-reduce-scatter fusion | flops 524289 | bytes 1704448
  262.8 3.3 collective-permute-start.36
  266.0 3.0 collective-permute-start.35
  269.0 3.5 collective-permute-start.34
  274.5 4.9 collective-permute-done.37
  280.4 4.0 multiply_add_fusion
  290.4 7.1 %reduce-scatter.16.cloned.1.call-done = bf16[6,1024]{1,0:T(8,128)(2,1)} async-done(((bf16[6,2048]{1,0:T(8,128)(2,1)}), bf16[6,1024]{1,0:T(8,128)(2,1)}) %reduce-scatter.16.cloned.1.call-update) | async-done | bytes 12304 | tf_op jit(solution)/shard_map/reduce_scatter | solution.py:107
  306.0 2.9 collective-permute-start.17
  313.6 3.5 collective-permute-done.18
  318.2 4.4 collective-permute-done.19
  322.9 5.3 %collective-permute-done.20 = bf16[6,1024]{1,0:T(8,128)(2,1)S(1)} collective-permute-done((bf16[6,1024]{1,0:T(8,128)(2,1)S(1)}, bf16[6,1024]{1,0:T(8,128)(2,1)S(1)}, u32[]{:S(2)}, u32[]{:S(2)}) %collective-permute-start.20) | collective-permute-done | bytes 12320 | tf_op jit(solution)/shard_map/ppermute | solution.py:15
  328.1 5.5 %collective-permute-done.21 = bf16[6,1024]{1,0:T(8,128)(2,1)S(1)} collective-permute-done((bf16[6,1024]{1,0:T(8,128)(2,1)S(1)}, bf16[6,1024]{1,0:T(8,128)(2,1)S(1)}, u32[]{:S(2)}, u32[]{:S(2)}) %collective-permute-start.21) | collective-permute-done | bytes 12320 | tf_op jit(solution)/shard_map/ppermute | solution.py:15
  333.7 5.5 %collective-permute-done.22 = bf16[6,1024]{1,0:T(8,128)(2,1)S(1)} collective-permute-done((bf16[6,1024]{1,0:T(8,128)(2,1)S(1)}, bf16[6,1024]{1,0:T(8,128)(2,1)S(1)}, u32[]{:S(2)}, u32[]{:S(2)}) %collective-permute-start.22) | collective-permute-done | bytes 12320 | tf_op jit(solution)/shard_map/ppermute | solution.py:15
  339.2 5.6 %collective-permute-done.23 = bf16[6,1024]{1,0:T(8,128)(2,1)S(1)} collective-permute-done((bf16[6,1024]{1,0:T(8,128)(2,1)S(1)}, bf16[6,1024]{1,0:T(8,128)(2,1)S(1)}, u32[]{:S(2)}, u32[]{:S(2)}) %collective-permute-start.23) | collective-permute-done | bytes 12320 | tf_op jit(solution)/shard_map/ppermute | solution.py:15
  344.8 5.5 %collective-permute-done.24 = bf16[6,1024]{1,0:T(8,128)(2,1)S(1)} collective-permute-done((bf16[6,1024]{1,0:T(8,128)(2,1)S(1)}, bf16[6,1024]{1,0:T(8,128)(2,1)S(1)}, u32[]{:S(2)}, u32[]{:S(2)}) %collective-permute-start.24) | collective-permute-done | bytes 12320 | tf_op jit(solution)/shard_map/ppermute | solution.py:15
  350.4 5.5 %collective-permute-done.25 = bf16[6,1024]{1,0:T(8,128)(2,1)S(1)} collective-permute-done((bf16[6,1024]{1,0:T(8,128)(2,1)S(1)}, bf16[6,1024]{1,0:T(8,128)(2,1)S(1)}, u32[]{:S(2)}, u32[]{:S(2)}) %collective-permute-start.25) | collective-permute-done | bytes 12320 | tf_op jit(solution)/shard_map/ppermute | solution.py:15
  355.9 5.5 %collective-permute-done.26 = bf16[6,1024]{1,0:T(8,128)(2,1)S(1)} collective-permute-done((bf16[6,1024]{1,0:T(8,128)(2,1)S(1)}, bf16[6,1024]{1,0:T(8,128)(2,1)S(1)}, u32[]{:S(2)}, u32[]{:S(2)}) %collective-permute-start.26) | collective-permute-done | bytes 12320 | tf_op jit(solution)/shard_map/ppermute | solution.py:15
  361.4 5.6 %collective-permute-done.27 = bf16[6,1024]{1,0:T(8,128)(2,1)S(1)} collective-permute-done((bf16[6,1024]{1,0:T(8,128)(2,1)S(1)}, bf16[6,1024]{1,0:T(8,128)(2,1)S(1)}, u32[]{:S(2)}, u32[]{:S(2)}) %collective-permute-start.27) | collective-permute-done | bytes 12320 | tf_op jit(solution)/shard_map/ppermute | solution.py:15
  367.3 5.3 %collective-permute-done.28 = bf16[6,1024]{1,0:T(8,128)(2,1)S(1)} collective-permute-done((bf16[6,1024]{1,0:T(8,128)(2,1)S(1)}, bf16[6,1024]{1,0:T(8,128)(2,1)S(1)}, u32[]{:S(2)}, u32[]{:S(2)}) %collective-permute-start.28) | collective-permute-done | bytes 12320 | tf_op jit(solution)/shard_map/ppermute | solution.py:15
  374.6 3.5 collective-permute-done.29
  384.0 30.1 %reduce-scatter.18.cloned.1.call-done = bf16[48,352]{1,0:T(8,128)(2,1)} async-done(((bf16[96,352]{1,0:T(8,128)(2,1)}), bf16[48,352]{1,0:T(8,128)(2,1)}) %reduce-scatter.18.cloned.1.call-update) | async-done | bytes 33808 | tf_op jit(solution)/shard_map/reduce_scatter | solution.py:29
  414.1 10.7 %reduce-scatter.20.cloned.1.call-done = bf16[48,352]{1,0:T(8,128)(2,1)} async-done(((bf16[96,352]{1,0:T(8,128)(2,1)}), bf16[48,352]{1,0:T(8,128)(2,1)}) %reduce-scatter.20.cloned.1.call-update) | async-done | bytes 33808 | tf_op jit(solution)/shard_map/reduce_scatter | solution.py:32
  427.9 35.6 %fusion.2 = f32[8,1024]{1,0:T(8,128)S(1)} fusion(f32[96,1024]{1,0:T(8,128)S(1)} %fusion.49), kind=kCustom, calls=%all-reduce-scatter.2 | all-reduce-scatter fusion | flops 131073 | bytes 426496
  463.4 6.0 %collective-permute-start.40 = (f32[8,1024]{1,0:T(8,128)S(1)}, f32[8,1024]{1,0:T(8,128)S(1)}, u32[]{:S(2)}, u32[]{:S(2)}) collective-permute-start(f32[8,1024]{1,0:T(8,128)S(1)} %fusion.2), channel_id=1, source_target_pairs={{0,6},{2,8},{4,10},{6,12},{8,14},{10,16},{12,18},{14,20},{16,22},{... | collective-permute-start | bytes 98312
  469.4 4.4 collective-permute-start.39
  473.8 4.9 collective-permute-start.38
  480.6 3.9 collective-permute-done.41
  (129 shorter events, 77.2 us)
Async XLA Ops:
  7.2 118.1 %reduce-scatter.12.cloned.1.call-start = ((), (), s32[]{:S(2)}) async-start(), calls=%async_computation.6 | async-start | bytes 110592 | tf_op jit(solution)/shard_map/reduce_scatter | solution.py:29
  7.3 4.0 collective-permute-start
  11.3 4.0 collective-permute-start.1
  15.3 5.5 %collective-permute-start.2 = (bf16[6,1024]{1,0:T(8,128)(2,1)S(1)}, bf16[6,1024]{1,0:T(8,128)(2,1)S(1)}, u32[]{:S(2)}, u32[]{:S(2)}) collective-permute-start(bf16[6,1024]{1,0:T(8,128)(2,1)S(1)} %collective-permute-done.1), channel_id=1, source_target_pairs={{0,2},{2,4},{4,6},{6,8},{8,10},{10,12},{12,14},{14,16},{16,18},{18... | collective-permute-start | bytes 36872 | tf_op jit(solution)/shard_map/ppermute | solution.py:15
  20.9 5.6 %collective-permute-start.3 = (bf16[6,1024]{1,0:T(8,128)(2,1)S(1)}, bf16[6,1024]{1,0:T(8,128)(2,1)S(1)}, u32[]{:S(2)}, u32[]{:S(2)}) collective-permute-start(bf16[6,1024]{1,0:T(8,128)(2,1)S(1)} %collective-permute-done.2), channel_id=1, source_target_pairs={{0,2},{2,4},{4,6},{6,8},{8,10},{10,12},{12,14},{14,16},{16,18},{18... | collective-permute-start | bytes 36872 | tf_op jit(solution)/shard_map/ppermute | solution.py:15
  26.5 5.4 %collective-permute-start.4 = (bf16[6,1024]{1,0:T(8,128)(2,1)S(1)}, bf16[6,1024]{1,0:T(8,128)(2,1)S(1)}, u32[]{:S(2)}, u32[]{:S(2)}) collective-permute-start(bf16[6,1024]{1,0:T(8,128)(2,1)S(1)} %collective-permute-done.3), channel_id=1, source_target_pairs={{0,2},{2,4},{4,6},{6,8},{8,10},{10,12},{12,14},{14,16},{16,18},{18... | collective-permute-start | bytes 36872 | tf_op jit(solution)/shard_map/ppermute | solution.py:15
  32.0 5.5 %collective-permute-start.5 = (bf16[6,1024]{1,0:T(8,128)(2,1)S(1)}, bf16[6,1024]{1,0:T(8,128)(2,1)S(1)}, u32[]{:S(2)}, u32[]{:S(2)}) collective-permute-start(bf16[6,1024]{1,0:T(8,128)(2,1)S(1)} %collective-permute-done.4), channel_id=1, source_target_pairs={{0,2},{2,4},{4,6},{6,8},{8,10},{10,12},{12,14},{14,16},{16,18},{18... | collective-permute-start | bytes 36872 | tf_op jit(solution)/shard_map/ppermute | solution.py:15
  37.5 5.5 %collective-permute-start.6 = (bf16[6,1024]{1,0:T(8,128)(2,1)S(1)}, bf16[6,1024]{1,0:T(8,128)(2,1)S(1)}, u32[]{:S(2)}, u32[]{:S(2)}) collective-permute-start(bf16[6,1024]{1,0:T(8,128)(2,1)S(1)} %collective-permute-done.5), channel_id=1, source_target_pairs={{0,2},{2,4},{4,6},{6,8},{8,10},{10,12},{12,14},{14,16},{16,18},{18... | collective-permute-start | bytes 36872 | tf_op jit(solution)/shard_map/ppermute | solution.py:15
  43.0 5.6 %collective-permute-start.7 = (bf16[6,1024]{1,0:T(8,128)(2,1)S(1)}, bf16[6,1024]{1,0:T(8,128)(2,1)S(1)}, u32[]{:S(2)}, u32[]{:S(2)}) collective-permute-start(bf16[6,1024]{1,0:T(8,128)(2,1)S(1)} %collective-permute-done.6), channel_id=1, source_target_pairs={{0,2},{2,4},{4,6},{6,8},{8,10},{10,12},{12,14},{14,16},{16,18},{18... | collective-permute-start | bytes 36872 | tf_op jit(solution)/shard_map/ppermute | solution.py:15
  48.6 5.5 %collective-permute-start.8 = (bf16[6,1024]{1,0:T(8,128)(2,1)S(1)}, bf16[6,1024]{1,0:T(8,128)(2,1)S(1)}, u32[]{:S(2)}, u32[]{:S(2)}) collective-permute-start(bf16[6,1024]{1,0:T(8,128)(2,1)S(1)} %collective-permute-done.7), channel_id=1, source_target_pairs={{0,2},{2,4},{4,6},{6,8},{8,10},{10,12},{12,14},{14,16},{16,18},{18... | collective-permute-start | bytes 36872 | tf_op jit(solution)/shard_map/ppermute | solution.py:15
  54.1 5.5 %collective-permute-start.9 = (bf16[6,1024]{1,0:T(8,128)(2,1)S(1)}, bf16[6,1024]{1,0:T(8,128)(2,1)S(1)}, u32[]{:S(2)}, u32[]{:S(2)}) collective-permute-start(bf16[6,1024]{1,0:T(8,128)(2,1)S(1)} %collective-permute-done.8), channel_id=1, source_target_pairs={{0,2},{2,4},{4,6},{6,8},{8,10},{10,12},{12,14},{14,16},{16,18},{18... | collective-permute-start | bytes 36872 | tf_op jit(solution)/shard_map/ppermute | solution.py:15
  59.6 5.5 %collective-permute-start.10 = (bf16[6,1024]{1,0:T(8,128)(2,1)S(1)}, bf16[6,1024]{1,0:T(8,128)(2,1)S(1)}, u32[]{:S(2)}, u32[]{:S(2)}) collective-permute-start(bf16[6,1024]{1,0:T(8,128)(2,1)S(1)} %collective-permute-done.9), channel_id=1, source_target_pairs={{0,2},{2,4},{4,6},{6,8},{8,10},{10,12},{12,14},{14,16},{16,18},{18... | collective-permute-start | bytes 36872 | tf_op jit(solution)/shard_map/ppermute | solution.py:15
  65.2 5.5 %collective-permute-start.11 = (bf16[6,1024]{1,0:T(8,128)(2,1)S(1)}, bf16[6,1024]{1,0:T(8,128)(2,1)S(1)}, u32[]{:S(2)}, u32[]{:S(2)}) collective-permute-start(bf16[6,1024]{1,0:T(8,128)(2,1)S(1)} %collective-permute-done.10), channel_id=1, source_target_pairs={{0,2},{2,4},{4,6},{6,8},{8,10},{10,12},{12,14},{14,16},{16,18},{18... | collective-permute-start | bytes 36872 | tf_op jit(solution)/shard_map/ppermute | solution.py:15
  70.7 5.5 %collective-permute-start.12 = (bf16[6,1024]{1,0:T(8,128)(2,1)S(1)}, bf16[6,1024]{1,0:T(8,128)(2,1)S(1)}, u32[]{:S(2)}, u32[]{:S(2)}) collective-permute-start(bf16[6,1024]{1,0:T(8,128)(2,1)S(1)} %collective-permute-done.11), channel_id=1, source_target_pairs={{0,2},{2,4},{4,6},{6,8},{8,10},{10,12},{12,14},{14,16},{16,18},{18... | collective-permute-start | bytes 36872 | tf_op jit(solution)/shard_map/ppermute | solution.py:15
  76.3 5.5 %collective-permute-start.13 = (bf16[6,1024]{1,0:T(8,128)(2,1)S(1)}, bf16[6,1024]{1,0:T(8,128)(2,1)S(1)}, u32[]{:S(2)}, u32[]{:S(2)}) collective-permute-start(bf16[6,1024]{1,0:T(8,128)(2,1)S(1)} %collective-permute-done.12), channel_id=1, source_target_pairs={{0,2},{2,4},{4,6},{6,8},{8,10},{10,12},{12,14},{14,16},{16,18},{18... | collective-permute-start | bytes 36872 | tf_op jit(solution)/shard_map/ppermute | solution.py:15
  81.8 5.5 %collective-permute-start.14 = (bf16[6,1024]{1,0:T(8,128)(2,1)S(1)}, bf16[6,1024]{1,0:T(8,128)(2,1)S(1)}, u32[]{:S(2)}, u32[]{:S(2)}) collective-permute-start(bf16[6,1024]{1,0:T(8,128)(2,1)S(1)} %collective-permute-done.13), channel_id=1, source_target_pairs={{0,2},{2,4},{4,6},{6,8},{8,10},{10,12},{12,14},{14,16},{16,18},{18... | collective-permute-start | bytes 36872 | tf_op jit(solution)/shard_map/ppermute | solution.py:15
  91.4 45.4 %reduce-scatter.14.cloned.1.call-start = ((), (), s32[]{:S(2)}) async-start(), calls=%async_computation.7 | async-start | bytes 110592 | tf_op jit(solution)/shard_map/reduce_scatter | solution.py:32
  175.4 21.1 %collective-permute-start.32 = (f32[8,1024]{1,0:T(8,128)S(1)}, f32[8,1024]{1,0:T(8,128)S(1)}, u32[]{:S(2)}, u32[]{:S(2)}) collective-permute-start(f32[8,1024]{1,0:T(8,128)S(1)} %fusion), channel_id=1, source_target_pairs={{0,6},{2,8},{4,10},{6,12},{8,14},{10,16},{12,18},{14,20},{16,22},{... | collective-permute-start | bytes 98312
  181.4 15.1 %collective-permute-start.31 = (f32[8,1024]{1,0:T(8,128)S(1)}, f32[8,1024]{1,0:T(8,128)S(1)}, u32[]{:S(2)}, u32[]{:S(2)}) collective-permute-start(f32[8,1024]{1,0:T(8,128)S(1)} %fusion), channel_id=1, source_target_pairs={{0,4},{2,6},{4,8},{6,10},{8,12},{10,14},{12,16},{14,18},{16,20},{1... | collective-permute-start | bytes 98312
  185.8 10.7 %collective-permute-start.30 = (f32[8,1024]{1,0:T(8,128)S(1)}, f32[8,1024]{1,0:T(8,128)S(1)}, u32[]{:S(2)}, u32[]{:S(2)}) collective-permute-start(f32[8,1024]{1,0:T(8,128)S(1)} %fusion), channel_id=1, source_target_pairs={{0,2},{2,4},{4,6},{6,8},{8,10},{10,12},{12,14},{14,16},{16,18},{18... | collective-permute-start | bytes 98312
  190.7 5.8 %collective-permute-start.33 = (f32[6,1024]{1,0:T(8,128)S(1)}, f32[6,1024]{1,0:T(8,128)S(1)}, u32[]{:S(2)}, u32[]{:S(2)}) collective-permute-start(f32[6,1024]{1,0:T(8,128)S(1)} %slice.20), channel_id=1, source_target_pairs={{0,8},{2,10},{4,12},{6,14},{8,16},{10,18},{12,20},{14,22},{16,24},... | collective-permute-start | bytes 73736
  199.5 9.4 %all-to-all-start = ((bf16[6,16,128]{2,0,1:T(8,128)(2,1)}), bf16[6,16,128]{2,0,1:T(8,128)(2,1)S(1)}, u32[]{:S(2)}, u32[]{:S(2)}) async-start(bf16[6,16,128]{2,0,1:T(8,128)(2,1)} %get-tuple-element.11), calls=%async_computation.2 | async-start | bytes 65536 | tf_op jit(solution)/shard_map/all_to_all | solution.py:69
  204.7 92.8 %reduce-scatter.16.cloned.1.call-start = ((), (), s32[]{:S(2)}) async-start(), calls=%async_computation.8 | async-start | bytes 49152 | tf_op jit(solution)/shard_map/reduce_scatter | solution.py:107
  262.8 16.6 %collective-permute-start.36 = (f32[8,4096]{1,0:T(8,128)S(1)}, f32[8,4096]{1,0:T(8,128)S(1)}, u32[]{:S(2)}, u32[]{:S(2)}) collective-permute-start(f32[8,4096]{1,0:T(8,128)S(1)} %fusion.1), channel_id=1, source_target_pairs={{0,6},{2,8},{4,10},{6,12},{8,14},{10,16},{12,18},{14,20},{16,22},{... | collective-permute-start | bytes 393224
  266.0 13.4 %collective-permute-start.35 = (f32[8,4096]{1,0:T(8,128)S(1)}, f32[8,4096]{1,0:T(8,128)S(1)}, u32[]{:S(2)}, u32[]{:S(2)}) collective-permute-start(f32[8,4096]{1,0:T(8,128)S(1)} %fusion.1), channel_id=1, source_target_pairs={{0,4},{2,6},{4,8},{6,10},{8,12},{10,14},{12,16},{14,18},{16,20},{1... | collective-permute-start | bytes 393224
  269.0 10.4 %collective-permute-start.34 = (f32[8,4096]{1,0:T(8,128)S(1)}, f32[8,4096]{1,0:T(8,128)S(1)}, u32[]{:S(2)}, u32[]{:S(2)}) collective-permute-start(f32[8,4096]{1,0:T(8,128)S(1)} %fusion.1), channel_id=1, source_target_pairs={{0,2},{2,4},{4,6},{6,8},{8,10},{10,12},{12,14},{14,16},{16,18},{18... | collective-permute-start | bytes 393224
  272.5 6.9 %collective-permute-start.37 = (f32[6,4096]{1,0:T(8,128)S(1)}, f32[6,4096]{1,0:T(8,128)S(1)}, u32[]{:S(2)}, u32[]{:S(2)}) collective-permute-start(f32[6,4096]{1,0:T(8,128)S(1)} %slice.21), channel_id=1, source_target_pairs={{0,8},{2,10},{4,12},{6,14},{8,16},{10,18},{12,20},{14,22},{16,24},... | collective-permute-start | bytes 294920
  290.3 123.8 %reduce-scatter.18.cloned.1.call-start = ((), (), s32[]{:S(2)}) async-start(), calls=%async_computation.9 | async-start | bytes 110592 | tf_op jit(solution)/shard_map/reduce_scatter | solution.py:29
  298.2 3.7 collective-permute-start.15
  301.9 4.1 collective-permute-start.16
  306.0 5.5 %collective-permute-start.17 = (bf16[6,1024]{1,0:T(8,128)(2,1)S(1)}, bf16[6,1024]{1,0:T(8,128)(2,1)S(1)}, u32[]{:S(2)}, u32[]{:S(2)}) collective-permute-start(bf16[6,1024]{1,0:T(8,128)(2,1)S(1)} %collective-permute-done.16), channel_id=1, source_target_pairs={{0,2},{2,4},{4,6},{6,8},{8,10},{10,12},{12,14},{14,16},{16,18},{18... | collective-permute-start | bytes 36872 | tf_op jit(solution)/shard_map/ppermute | solution.py:15
  311.5 5.5 %collective-permute-start.18 = (bf16[6,1024]{1,0:T(8,128)(2,1)S(1)}, bf16[6,1024]{1,0:T(8,128)(2,1)S(1)}, u32[]{:S(2)}, u32[]{:S(2)}) collective-permute-start(bf16[6,1024]{1,0:T(8,128)(2,1)S(1)} %collective-permute-done.17), channel_id=1, source_target_pairs={{0,2},{2,4},{4,6},{6,8},{8,10},{10,12},{12,14},{14,16},{16,18},{18... | collective-permute-start | bytes 36872 | tf_op jit(solution)/shard_map/ppermute | solution.py:15
  317.1 5.5 %collective-permute-start.19 = (bf16[6,1024]{1,0:T(8,128)(2,1)S(1)}, bf16[6,1024]{1,0:T(8,128)(2,1)S(1)}, u32[]{:S(2)}, u32[]{:S(2)}) collective-permute-start(bf16[6,1024]{1,0:T(8,128)(2,1)S(1)} %collective-permute-done.18), channel_id=1, source_target_pairs={{0,2},{2,4},{4,6},{6,8},{8,10},{10,12},{12,14},{14,16},{16,18},{18... | collective-permute-start | bytes 36872 | tf_op jit(solution)/shard_map/ppermute | solution.py:15
  322.6 5.5 %collective-permute-start.20 = (bf16[6,1024]{1,0:T(8,128)(2,1)S(1)}, bf16[6,1024]{1,0:T(8,128)(2,1)S(1)}, u32[]{:S(2)}, u32[]{:S(2)}) collective-permute-start(bf16[6,1024]{1,0:T(8,128)(2,1)S(1)} %collective-permute-done.19), channel_id=1, source_target_pairs={{0,2},{2,4},{4,6},{6,8},{8,10},{10,12},{12,14},{14,16},{16,18},{18... | collective-permute-start | bytes 36872 | tf_op jit(solution)/shard_map/ppermute | solution.py:15
  328.1 5.5 %collective-permute-start.21 = (bf16[6,1024]{1,0:T(8,128)(2,1)S(1)}, bf16[6,1024]{1,0:T(8,128)(2,1)S(1)}, u32[]{:S(2)}, u32[]{:S(2)}) collective-permute-start(bf16[6,1024]{1,0:T(8,128)(2,1)S(1)} %collective-permute-done.20), channel_id=1, source_target_pairs={{0,2},{2,4},{4,6},{6,8},{8,10},{10,12},{12,14},{14,16},{16,18},{18... | collective-permute-start | bytes 36872 | tf_op jit(solution)/shard_map/ppermute | solution.py:15
  333.7 5.5 %collective-permute-start.22 = (bf16[6,1024]{1,0:T(8,128)(2,1)S(1)}, bf16[6,1024]{1,0:T(8,128)(2,1)S(1)}, u32[]{:S(2)}, u32[]{:S(2)}) collective-permute-start(bf16[6,1024]{1,0:T(8,128)(2,1)S(1)} %collective-permute-done.21), channel_id=1, source_target_pairs={{0,2},{2,4},{4,6},{6,8},{8,10},{10,12},{12,14},{14,16},{16,18},{18... | collective-permute-start | bytes 36872 | tf_op jit(solution)/shard_map/ppermute | solution.py:15
  339.2 5.6 %collective-permute-start.23 = (bf16[6,1024]{1,0:T(8,128)(2,1)S(1)}, bf16[6,1024]{1,0:T(8,128)(2,1)S(1)}, u32[]{:S(2)}, u32[]{:S(2)}) collective-permute-start(bf16[6,1024]{1,0:T(8,128)(2,1)S(1)} %collective-permute-done.22), channel_id=1, source_target_pairs={{0,2},{2,4},{4,6},{6,8},{8,10},{10,12},{12,14},{14,16},{16,18},{18... | collective-permute-start | bytes 36872 | tf_op jit(solution)/shard_map/ppermute | solution.py:15
  344.8 5.5 %collective-permute-start.24 = (bf16[6,1024]{1,0:T(8,128)(2,1)S(1)}, bf16[6,1024]{1,0:T(8,128)(2,1)S(1)}, u32[]{:S(2)}, u32[]{:S(2)}) collective-permute-start(bf16[6,1024]{1,0:T(8,128)(2,1)S(1)} %collective-permute-done.23), channel_id=1, source_target_pairs={{0,2},{2,4},{4,6},{6,8},{8,10},{10,12},{12,14},{14,16},{16,18},{18... | collective-permute-start | bytes 36872 | tf_op jit(solution)/shard_map/ppermute | solution.py:15
  350.4 5.5 %collective-permute-start.25 = (bf16[6,1024]{1,0:T(8,128)(2,1)S(1)}, bf16[6,1024]{1,0:T(8,128)(2,1)S(1)}, u32[]{:S(2)}, u32[]{:S(2)}) collective-permute-start(bf16[6,1024]{1,0:T(8,128)(2,1)S(1)} %collective-permute-done.24), channel_id=1, source_target_pairs={{0,2},{2,4},{4,6},{6,8},{8,10},{10,12},{12,14},{14,16},{16,18},{18... | collective-permute-start | bytes 36872 | tf_op jit(solution)/shard_map/ppermute | solution.py:15
  355.9 5.5 %collective-permute-start.26 = (bf16[6,1024]{1,0:T(8,128)(2,1)S(1)}, bf16[6,1024]{1,0:T(8,128)(2,1)S(1)}, u32[]{:S(2)}, u32[]{:S(2)}) collective-permute-start(bf16[6,1024]{1,0:T(8,128)(2,1)S(1)} %collective-permute-done.25), channel_id=1, source_target_pairs={{0,2},{2,4},{4,6},{6,8},{8,10},{10,12},{12,14},{14,16},{16,18},{18... | collective-permute-start | bytes 36872 | tf_op jit(solution)/shard_map/ppermute | solution.py:15
  361.4 5.6 %collective-permute-start.27 = (bf16[6,1024]{1,0:T(8,128)(2,1)S(1)}, bf16[6,1024]{1,0:T(8,128)(2,1)S(1)}, u32[]{:S(2)}, u32[]{:S(2)}) collective-permute-start(bf16[6,1024]{1,0:T(8,128)(2,1)S(1)} %collective-permute-done.26), channel_id=1, source_target_pairs={{0,2},{2,4},{4,6},{6,8},{8,10},{10,12},{12,14},{14,16},{16,18},{18... | collective-permute-start | bytes 36872 | tf_op jit(solution)/shard_map/ppermute | solution.py:15
  367.1 5.5 %collective-permute-start.28 = (bf16[6,1024]{1,0:T(8,128)(2,1)S(1)}, bf16[6,1024]{1,0:T(8,128)(2,1)S(1)}, u32[]{:S(2)}, u32[]{:S(2)}) collective-permute-start(bf16[6,1024]{1,0:T(8,128)(2,1)S(1)} %collective-permute-done.27), channel_id=1, source_target_pairs={{0,2},{2,4},{4,6},{6,8},{8,10},{10,12},{12,14},{14,16},{16,18},{18... | collective-permute-start | bytes 36872 | tf_op jit(solution)/shard_map/ppermute | solution.py:15
  372.6 5.5 %collective-permute-start.29 = (bf16[6,1024]{1,0:T(8,128)(2,1)S(1)}, bf16[6,1024]{1,0:T(8,128)(2,1)S(1)}, u32[]{:S(2)}, u32[]{:S(2)}) collective-permute-start(bf16[6,1024]{1,0:T(8,128)(2,1)S(1)} %collective-permute-done.28), channel_id=1, source_target_pairs={{0,2},{2,4},{4,6},{6,8},{8,10},{10,12},{12,14},{14,16},{16,18},{18... | collective-permute-start | bytes 36872 | tf_op jit(solution)/shard_map/ppermute | solution.py:15
  380.4 44.4 %reduce-scatter.20.cloned.1.call-start = ((), (), s32[]{:S(2)}) async-start(), calls=%async_computation.10 | async-start | bytes 110592 | tf_op jit(solution)/shard_map/reduce_scatter | solution.py:32
  463.4 21.1 %collective-permute-start.40 = (f32[8,1024]{1,0:T(8,128)S(1)}, f32[8,1024]{1,0:T(8,128)S(1)}, u32[]{:S(2)}, u32[]{:S(2)}) collective-permute-start(f32[8,1024]{1,0:T(8,128)S(1)} %fusion.2), channel_id=1, source_target_pairs={{0,6},{2,8},{4,10},{6,12},{8,14},{10,16},{12,18},{14,20},{16,22},{... | collective-permute-start | bytes 98312
  469.4 15.1 %collective-permute-start.39 = (f32[8,1024]{1,0:T(8,128)S(1)}, f32[8,1024]{1,0:T(8,128)S(1)}, u32[]{:S(2)}, u32[]{:S(2)}) collective-permute-start(f32[8,1024]{1,0:T(8,128)S(1)} %fusion.2), channel_id=1, source_target_pairs={{0,4},{2,6},{4,8},{6,10},{8,12},{10,14},{12,16},{14,18},{16,20},{1... | collective-permute-start | bytes 98312
  473.8 10.7 %collective-permute-start.38 = (f32[8,1024]{1,0:T(8,128)S(1)}, f32[8,1024]{1,0:T(8,128)S(1)}, u32[]{:S(2)}, u32[]{:S(2)}) collective-permute-start(f32[8,1024]{1,0:T(8,128)S(1)} %fusion.2), channel_id=1, source_target_pairs={{0,2},{2,4},{4,6},{6,8},{8,10},{10,12},{12,14},{14,16},{16,18},{18... | collective-permute-start | bytes 98312
  478.7 5.8 %collective-permute-start.41 = (f32[6,1024]{1,0:T(8,128)S(1)}, f32[6,1024]{1,0:T(8,128)S(1)}, u32[]{:S(2)}, u32[]{:S(2)}) collective-permute-start(f32[6,1024]{1,0:T(8,128)S(1)} %slice.22), channel_id=1, source_target_pairs={{0,8},{2,10},{4,12},{6,14},{8,16},{10,18},{12,20},{14,22},{16,24},... | collective-permute-start | bytes 73736
  (14 other events, 1726.1 us)
Sparse Core Ops, SparseCore 0:
  91.6 33.6 reduce-scatter.11
  128.1 8.6 reduce-scatter.13
  290.5 6.9 reduce-scatter.15
  380.5 33.5 reduce-scatter.17
  416.1 8.6 reduce-scatter.19
